TPU v7x, 32 devices: a whole 2x2x4 slice. The times are simulated.
32 devices in a mesh: sp: 8 (over z, core), tp: 4 (over y, x).
Axes of the slice: x: 2, y: 2, z: 4, core: 2. Of those that a mesh axis runs over, the one named last changes fastest.
Arguments:
- layer_input: bfloat16 [2048, 2048], P('sp', 'tp'), may hold values from -6 to 6
- doc_ids: int32 [2048], P('sp'), may hold values from 0 to 1, never falling along the last dimension, each value on 1 to 1536 neighbouring positions
- routes: int32 [2048, 2], P('sp'), may hold values from 0 to 7, all different within a row; in each aligned block of 256 rows (0 to 255, 256 to 511, ...) at most 88 rows name the same one
- route_weight: float32 [2048, 2], P('sp'), may hold values from 0.2 to 2
- pool_weight: bfloat16 [4, 512, 512], replicated, may hold values from -0.25 to 0.25
- pool_scale: float32 [2048], replicated, may hold values from 0.1 to 1.9
- norm1_gain: float32 [2048], replicated, may hold values from 0.3 to 3
- norm1_bias: float32 [2048], replicated, may hold values from -3 to 3
- expert_gate: bfloat16 [8, 2048, 2048], P('sp', None, 'tp'), may hold values from -0.125 to 0.125
- expert_up: bfloat16 [8, 2048, 2048], P('sp', None, 'tp'), may hold values from -0.125 to 0.125
- expert_down: bfloat16 [8, 2048, 2048], P('sp', 'tp'), may hold values from -0.125 to 0.125
- shared_gate: bfloat16 [2048, 1024], P(None, 'tp'), may hold values from -0.125 to 0.125
- shared_up: bfloat16 [2048, 1024], P(None, 'tp'), may hold values from -0.125 to 0.125
- shared_down: bfloat16 [1024, 2048], P('tp'), may hold values from -0.1875 to 0.1875
- norm2_gain: float32 [2048], P('tp'), may hold values from 0.1 to 1.9
- norm2_bias: float32 [2048], P('tp'), may hold values from -3 to 3
Outputs:
- settled: bfloat16 [2048, 2048], P('sp', 'tp')
Inputs may be any that keep to these rules, and one draw needn't show every extreme that they name: `routes`: in each aligned block of 256 rows no expert is named by more than 88 picks, a bound that some block reaches. `doc_ids`: never falling along the positions; each document spans 1 to 1536 positions.
All inputs are finite; a program needn't handle non-finite values.
Results may differ from a plain program's by a relative error of at most 0.013.
Values may be sent and summed in bfloat16 or wider, within the bound.
A program may use at most 64 MiB of HBM per device.

v0:
```python
import functools

import jax
import jax.numpy as jnp
from jax import lax
from jax.experimental import pallas as pl
from jax.experimental.pallas import tpu as pltpu
from jax.sharding import PartitionSpec as P

WINDOWS = (2, 4, 8, 16)
HALO_ROWS = 15
RESIDUAL_SCALE = 2.0**0.5
NORM_EPS = 1e-05


def shifted(shard, axis, by):
    size = lax.axis_size(axis)
    pairs = [(i, i + by) for i in range(size) if 0 <= i + by < size]
    return lax.ppermute(shard, axis, pairs)


def pooled_groups(extended, marks, halo_rows):
    length = extended.shape[0] - halo_rows
    group_width = extended.shape[1] // len(WINDOWS)
    own_mark = marks[halo_rows:]
    values = extended.astype(jnp.float32)
    outputs = []
    for group_index, window in enumerate(WINDOWS):
        section = values[:, group_index * group_width : (group_index + 1) * group_width]
        running = jnp.zeros((length, group_width), jnp.float32)
        members = jnp.zeros((length, 1), jnp.float32)
        for offset in range(window):
            first_row = halo_rows - offset
            inside = (marks[first_row : first_row + length] == own_mark).astype(jnp.float32)[
                :, None
            ]
            running = running + inside * section[first_row : first_row + length]
            members = members + inside
        outputs.append(running / members - section[halo_rows:])
    return jnp.concatenate(outputs, axis=1).astype(jnp.bfloat16)


def layer_norm_rows(values, gain, bias):
    row_mean = jnp.mean(values, axis=1, keepdims=True)
    row_var = jnp.mean(values * values, axis=1, keepdims=True) - row_mean * row_mean
    return (values - row_mean) * lax.rsqrt(row_var + NORM_EPS) * gain + bias


def shards(
    layer_input,
    doc_ids,
    routes,
    route_weight,
    pool_weight,
    pool_scale,
    norm1_gain,
    norm1_bias,
    expert_gate,
    expert_up,
    expert_down,
    shared_gate,
    shared_up,
    shared_down,
    norm2_gain,
    norm2_bias,
):
    tokens_here = layer_input.shape[0]
    width_here = layer_input.shape[1]
    doc_marks = (doc_ids + 1).astype(jnp.bfloat16)
    tail_rows, tail_marks = shifted(
        (layer_input[tokens_here - HALO_ROWS :], doc_marks[tokens_here - HALO_ROWS :]), "sp", 1
    )
    extended = jnp.concatenate([tail_rows, layer_input], axis=0)
    marks = jnp.concatenate([tail_marks, doc_marks]).astype(jnp.float32)
    whole = lax.all_gather(extended, "tp", axis=1, tiled=True)
    model_width = whole.shape[1]
    mixed = pooled_groups(whole, marks, HALO_ROWS)
    groups = pool_weight.shape[0]
    group_width = pool_weight.shape[1]
    projected = jnp.einsum(
        "tgc,gcd->tgd",
        mixed.reshape(tokens_here, groups, group_width),
        pool_weight,
        preferred_element_type=jnp.float32,
    ).reshape(tokens_here, model_width)
    first = RESIDUAL_SCALE * whole[HALO_ROWS:].astype(jnp.float32) + projected * pool_scale
    normed = layer_norm_rows(first, norm1_gain, norm1_bias).astype(jnp.bfloat16)
    top = routes.shape[1]
    experts_all = lax.axis_size("sp")
    capacity = (tokens_here * top * 11 + 8 * experts_all - 1) // (8 * experts_all)
    flat_routes = routes.reshape(-1)
    one_hot = (flat_routes[:, None] == jnp.arange(experts_all, dtype=jnp.int32)[None, :]).astype(
        jnp.int32
    )
    ranks = jnp.sum((jnp.cumsum(one_hot, axis=0) - one_hot) * one_hot, axis=1)
    destination = flat_routes * capacity + ranks
    picked_rows = jnp.repeat(normed, top, axis=0)
    send_buffer = (
        jnp.zeros((experts_all * capacity, model_width), jnp.bfloat16)
        .at[destination]
        .set(picked_rows)
    )
    slot_grid = send_buffer.reshape(experts_all, capacity, model_width)
    own_columns = lax.dynamic_slice_in_dim(
        slot_grid, lax.axis_index("tp") * width_here, width_here, 2
    )
    moved = lax.all_to_all(own_columns, "sp", split_axis=0, concat_axis=0, tiled=True)
    arrived = lax.all_gather(moved, "tp", axis=2, tiled=True)
    arrived_rows = arrived.reshape(-1, model_width)
    gate_part = jnp.dot(arrived_rows, expert_gate[0], preferred_element_type=jnp.float32)
    up_part = jnp.dot(arrived_rows, expert_up[0], preferred_element_type=jnp.float32)
    expert_hidden = (jax.nn.silu(gate_part) * up_part).astype(jnp.bfloat16)
    routed_partial = jnp.dot(expert_hidden, expert_down[0], preferred_element_type=jnp.float32)
    shared_gate_part = jnp.dot(normed, shared_gate, preferred_element_type=jnp.float32)
    shared_up_part = jnp.dot(normed, shared_up, preferred_element_type=jnp.float32)
    shared_hidden = (jax.nn.silu(shared_gate_part) * shared_up_part).astype(jnp.bfloat16)
    shared_partial = jnp.dot(shared_hidden, shared_down, preferred_element_type=jnp.float32)
    routed_sum, shared_sum = (
        lax.psum_scatter(
            routed_partial.astype(jnp.bfloat16), "tp", scatter_dimension=1, tiled=True
        ).astype(jnp.float32),
        lax.psum_scatter(
            shared_partial.astype(jnp.bfloat16), "tp", scatter_dimension=1, tiled=True
        ).astype(jnp.float32),
    )
    routed_here = routed_sum.astype(jnp.bfloat16).reshape(experts_all, capacity, width_here)
    returned = lax.all_to_all(routed_here, "sp", split_axis=0, concat_axis=0, tiled=True)
    returned_rows = returned.reshape(experts_all * capacity, width_here)
    picked_out = (
        returned_rows[destination].astype(jnp.float32).reshape(tokens_here, top, width_here)
    )
    routed_mix = jnp.sum(picked_out * route_weight[:, :, None], axis=1)
    own_normed = lax.dynamic_slice_in_dim(
        normed, lax.axis_index("tp") * width_here, width_here, 1
    ).astype(jnp.float32)
    second = RESIDUAL_SCALE * own_normed + routed_mix + shared_sum
    row_total, row_squares = lax.psum(
        (jnp.sum(second, axis=1), jnp.sum(second * second, axis=1)), "tp"
    )
    row_mean = row_total / model_width
    row_var = row_squares / model_width - row_mean * row_mean
    scaled = (second - row_mean[:, None]) * lax.rsqrt(row_var + NORM_EPS)[:, None]
    return (scaled * norm2_gain + norm2_bias).astype(jnp.bfloat16)


MESH_ID = pl.DeviceIdType.MESH
HALO = 16
LANES = 128
F32 = jnp.float32
BF16 = jnp.bfloat16


def fused_kernel(
    dims,
    x_ref,
    cols_ref,
    par_ref,
    pool_hbm,
    gate_hbm,
    up_hbm,
    down_hbm,
    sgate_hbm,
    sup_hbm,
    sdown_hbm,
    out_ref,
    pool_w,
    gate_w,
    up_w,
    down_w,
    sgate_w,
    sup_w,
    sdown_w,
    halo_x,
    halo_c,
    disp,
    wsend,
    wrecv,
    stat_send,
    stat_recv,
    normed_ref,
    sbuf,
    xs,
    pbuf,
    pown,
    rdx,
    rdy,
    fx,
    fy,
    rsend,
    rback,
    send_sems,
    recv_sems,
    load_sems,
):
    experts, tps, cap, pad, windows = dims
    rows, width = x_ref.shape
    half = width // 2
    chips = experts // 2
    model_width = width * tps
    sp = lax.axis_index("sp")
    tp = lax.axis_index("tp")
    chip = sp // 2
    core = sp % 2
    xn = tp + 1 - 2 * (tp % 2)
    yn = lax.rem(tp + 2, tps)
    diag = xn + 2 - 4 * (xn // 2)
    at_q = (tp, xn, yn, diag)

    def forward(j):
        return lax.rem(chip + j // 2, chips) * 2 + (core if j % 2 == 0 else 1 - core)

    def backward(j):
        return lax.rem(chip + chips - j // 2, chips) * 2 + (core if j % 2 == 0 else 1 - core)

    counter = [0]

    def remote(src, dst, device):
        k = counter[0]
        counter[0] += 1
        return pltpu.make_async_remote_copy(
            src_ref=src,
            dst_ref=dst,
            send_sem=send_sems.at[k],
            recv_sem=recv_sems.at[k],
            device_id=device,
            device_id_type=MESH_ID,
        )

    loads = {}
    load_count = [0]

    def load(name, src, dst):
        k = load_count[0]
        load_count[0] += 1
        copy = pltpu.make_async_copy(src, dst, load_sems.at[k])
        copy.start()
        loads.setdefault(name, []).append(copy)

    load("pool", pool_hbm.at[tp], pool_w)
    for q in range(tps):
        block = pl.ds(pl.multiple_of(at_q[q] * width, width), width)
        load("in", gate_hbm.at[0, block, :], gate_w.at[q])
        load("in", up_hbm.at[0, block, :], up_w.at[q])
        load("in", sgate_hbm.at[block, :], sgate_w.at[q])
        load("in", sup_hbm.at[block, :], sup_w.at[q])
        load("down", down_hbm.at[0, :, block], down_w.at[q])
        load("down", sdown_hbm.at[:, block], sdown_w.at[q])

    barrier = pltpu.get_barrier_semaphore()
    for q in range(1, tps):
        pl.semaphore_signal(barrier, inc=1, device_id=(sp, at_q[q]), device_id_type=MESH_ID)
    for j in range(1, experts):
        pl.semaphore_signal(barrier, inc=1, device_id=(forward(j), tp), device_id_type=MESH_ID)
    pl.semaphore_wait(barrier, tps - 1 + experts - 1)

    following = lax.rem(sp + 1, experts)
    halo_copies = [
        remote(x_ref.at[pl.ds(rows - HALO, HALO)], halo_x, (following, tp)),
        remote(cols_ref.at[pl.ds(rows - HALO, HALO)], halo_c, (following, tp)),
    ]
    for copy in halo_copies:
        copy.start()

    cols = cols_ref[...]
    lane = lax.broadcasted_iota(jnp.int32, (rows, LANES), 1)
    route = [cols[:, 1 + k : 2 + k].astype(jnp.int32) for k in range(2)]
    weight = [cols[:, 3 + k : 4 + k] for k in range(2)]
    named = [lane == route[k] for k in range(2)]
    count = named[0].astype(F32) + named[1].astype(F32)
    earlier = (
        lax.broadcasted_iota(jnp.int32, (rows, rows), 0)
        > lax.broadcasted_iota(jnp.int32, (rows, rows), 1)
    ).astype(F32)
    rank = jnp.dot(earlier.astype(BF16), count.astype(BF16), preferred_element_type=F32)
    lane_chip = lane // 2
    ahead = jnp.where(lane_chip < chip, lane_chip - chip + chips, lane_chip - chip)
    differs = jnp.where(lane % 2 == core, 0, 1)
    place = (rank + 0.5).astype(jnp.int32) + (ahead * 2 + differs) * pad
    dest = [
        jnp.sum(jnp.where(named[k], place, 0).astype(F32), axis=1, keepdims=True) for k in range(2)
    ]
    both = jnp.where(lane == 0, dest[0], jnp.where(lane == 1, dest[1], 0.0))
    both_rows = both.T
    slot_row = lax.broadcasted_iota(jnp.int32, (experts * pad, rows), 0)
    dest_row = [(both_rows[k : k + 1, :] + 0.5).astype(jnp.int32) for k in range(2)]
    disp[...] = jnp.where(
        (slot_row == dest_row[0]) | (slot_row == dest_row[1]), 1.0, 0.0
    ).astype(BF16)
    dest_col = [(dest[k] + 0.5).astype(jnp.int32) for k in range(2)]
    sub = lax.broadcasted_iota(jnp.int32, (8, LANES), 0)
    for j in range(experts):
        first_here = dest_col[0] == lane + j * pad
        second_here = dest_col[1] == lane + j * pad
        slot_weight = jnp.sum(
            jnp.where(first_here, weight[0], jnp.where(second_here, weight[1], 0.0)),
            axis=0,
            keepdims=True,
        )
        slot_flag = jnp.sum(jnp.where(first_here, 1.0, 0.0), axis=0, keepdims=True)
        tile = jnp.where(sub == 0, slot_weight, jnp.where(sub == 1, slot_flag, 0.0))
        if j == 0:
            wrecv[0] = tile
        else:
            wsend[j] = tile
    weight_copies = {}
    for j in range(1, experts):
        weight_copies[j] = remote(wsend.at[j], wrecv.at[j], (forward(j), tp))
        weight_copies[j].start()

    for copy in halo_copies:
        copy.wait_recv()
    value = x_ref[...].astype(F32)
    running = jnp.concatenate([halo_x[...].astype(F32), value], axis=0)
    halo_docs = jnp.where(sp == 0, -1.0, halo_c[...][:, 0:1])
    docs = jnp.concatenate([halo_docs, cols[:, 0:1]], axis=0)
    docs = jnp.broadcast_to(docs, (rows + HALO, LANES))
    members = jnp.ones((rows + HALO, LANES), F32)
    window = jnp.int32(windows[0])
    for index in range(1, len(windows)):
        window = jnp.where(tp == index, windows[index], window)
    step = 1
    while step < max(windows):
        same = (docs == pltpu.roll(docs, step, 0)) & (step < window)
        keep = same[:, 0:1]
        running = running + jnp.where(keep, pltpu.roll(running, step, 0), 0.0)
        members = members + jnp.where(same, pltpu.roll(members, step, 0), 0.0)
        step *= 2
    mixed = (running[HALO:] / members[HALO:, 0:1] - value).astype(BF16)
    for copy in loads["pool"]:
        copy.wait()
    projected = jnp.dot(mixed, pool_w[...], preferred_element_type=F32)
    par = par_ref[...]
    first = (2.0**0.5) * value + projected * par[0:1]

    def exchange(values, slot):
        total = jnp.sum(values, axis=1, keepdims=True)
        squares = jnp.sum(values * values, axis=1, keepdims=True)
        tile = jnp.where(lane == 0, total, jnp.where(lane == 1, squares, 0.0))
        own = tile.T[0:8]
        stat_send[slot] = own
        copies = []
        for q in range(1, tps):
            copies.append(remote(stat_send.at[slot], stat_recv.at[slot, q], (sp, at_q[q])))
            copies[-1].start()
        for copy in copies:
            copy.wait_recv()
        for q in range(1, tps):
            own = own + stat_recv[slot, q]
        back = own.T
        mean = back[:, 0:1] / model_width
        var = back[:, 1:2] / model_width - mean * mean
        return mean, lax.rsqrt(var + 1e-5), copies

    mean, inverse, stat_copies = exchange(first, 0)
    normed = ((first - mean) * inverse * par[1:2] + par[2:3]).astype(BF16)
    normed_ref[...] = normed

    moves = {}
    groups = chips
    for c in list(range(1, groups)) + [0]:
        part = jnp.dot(
            disp[c * 2 * pad : (c + 1) * 2 * pad, :], normed, preferred_element_type=F32
        ).astype(BF16)
        for b in range(2):
            j = 2 * c + b
            piece = part[b * pad : (b + 1) * pad]
            if j == 0:
                xs[0, 0] = piece
            else:
                sbuf[j] = piece
                moves[j] = remote(
                    sbuf.at[j, pl.ds(0, cap)], xs.at[0, j, pl.ds(0, cap)], (forward(j), tp)
                )
                moves[j].start()

    to_x, to_y, via_x, via_y = {}, {}, {}, {}
    half_x, half_y, full_x, full_y = {}, {}, {}, {}
    back = {}

    def pair(ref, q, c, columns=None):
        if columns is None:
            return ref.at[q, pl.ds(2 * c, 2), pl.ds(0, cap)]
        return ref.at[q, pl.ds(2 * c, 2), pl.ds(0, cap), columns]

    low, high = pl.ds(0, half), pl.ds(half, half)

    def stage_gather(c):
        for b in range(2):
            if 2 * c + b:
                moves[2 * c + b].wait_recv()
                weight_copies[2 * c + b].wait_recv()
        to_x[c] = remote(pair(xs, 0, c), pair(xs, 1, c), (sp, xn))
        to_x[c].start()
        to_y[c] = remote(pair(xs, 0, c), pair(xs, 2, c), (sp, yn))
        to_y[c].start()

    def stage_relay(c):
        to_x[c].wait_recv()
        via_y[c] = remote(pair(xs, 1, c, low), pair(xs, 3, c, low), (sp, yn))
        via_y[c].start()
        to_y[c].wait_recv()
        via_x[c] = remote(pair(xs, 2, c, high), pair(xs, 3, c, high), (sp, xn))
        via_x[c].start()

    def stage_expert(c):
        via_x[c].wait_recv()
        via_y[c].wait_recv()
        if c == 0:
            for copy in loads["in"]:
                copy.wait()
        size = 2 * pad
        tiles = [wrecv[2 * c + b].T[0:pad] for b in range(2)]
        slot = jnp.concatenate(tiles, axis=0)
        acts = [xs[q, 2 * c : 2 * c + 2].reshape(size, width) for q in range(tps)]

        def project(w):
            total = jnp.dot(acts[0], w[0], preferred_element_type=F32)
            for q in range(1, tps):
                total = total + jnp.dot(acts[q], w[q], preferred_element_type=F32)
            return total

        hidden = (jax.nn.silu(project(gate_w)) * project(up_w) * slot[:, 0:1]).astype(BF16)
        shared = (jax.nn.silu(project(sgate_w)) * project(sup_w) * slot[:, 1:2]).astype(BF16)
        if c == 0:
            for copy in loads["down"]:
                copy.wait()

        def partial(q):
            return jnp.dot(hidden, down_w[q], preferred_element_type=F32) + jnp.dot(
                shared, sdown_w[q], preferred_element_type=F32
            )

        pbuf[3, 2 * c : 2 * c + 2] = partial(3).astype(BF16).reshape(2, pad, width)
        half_x[c] = remote(
            pair(pbuf, 3, c, low), rdx.at[pl.ds(2 * c, 2), pl.ds(0, cap)], (sp, xn)
        )
        half_x[c].start()
        half_y[c] = remote(
            pair(pbuf, 3, c, high), rdy.at[pl.ds(2 * c, 2), pl.ds(0, cap)], (sp, yn)
        )
        half_y[c].start()
        pbuf[1, 2 * c : 2 * c + 2] = partial(1).astype(BF16).reshape(2, pad, width)
        pbuf[2, 2 * c : 2 * c + 2] = partial(2).astype(BF16).reshape(2, pad, width)
        pown[2 * c : 2 * c + 2] = partial(0).reshape(2, pad, width)

    def stage_fold(c):
        two = slice(2 * c, 2 * c + 2)
        half_x[c].wait_recv()
        pbuf[2, two, :, :half] = (
            pbuf[2, two, :, :half].astype(F32) + rdx[two].astype(F32)
        ).astype(BF16)
        full_y[c] = remote(pair(pbuf, 2, c), fy.at[pl.ds(2 * c, 2), pl.ds(0, cap)], (sp, yn))
        full_y[c].start()
        half_y[c].wait_recv()
        pbuf[1, two, :, half:] = (
            pbuf[1, two, :, half:].astype(F32) + rdy[two].astype(F32)
        ).astype(BF16)
        full_x[c] = remote(pair(pbuf, 1, c), fx.at[pl.ds(2 * c, 2), pl.ds(0, cap)], (sp, xn))
        full_x[c].start()

    def stage_return(c):
        two = slice(2 * c, 2 * c + 2)
        full_x[c].wait_recv()
        full_y[c].wait_recv()
        total = (pown[two] + fx[two].astype(F32) + fy[two].astype(F32)).astype(BF16)
        for b in range(2):
            j = 2 * c + b
            if j == 0:
                rback[0] = total[0]
            else:
                rsend[j] = total[b]
                back[j] = remote(
                    rsend.at[j, pl.ds(0, cap)], rback.at[j, pl.ds(0, cap)], (backward(j), tp)
                )
                back[j].start()

    stages = (stage_gather, stage_relay, stage_expert, stage_fold, stage_return)
    for tick in range(groups + len(stages) - 1):
        for depth, stage in enumerate(stages):
            if 0 <= tick - depth < groups:
                stage(tick - depth)

    for j in range(1, experts):
        back[j].wait_recv()
    slots = rback[...].reshape(experts * pad, width)
    inner = lax.broadcasted_iota(jnp.int32, (experts, pad, width), 1).reshape(
        experts * pad, width
    )
    slots = jnp.where(inner < cap, slots.astype(F32), 0.0).astype(BF16)
    mix = lax.dot_general(
        disp[...], slots, (((0,), (0,)), ((), ())), preferred_element_type=F32
    )
    second = (2.0**0.5) * normed_ref[...].astype(F32) + mix
    mean2, inverse2, stat_copies2 = exchange(second, 1)
    out_ref[...] = ((second - mean2) * inverse2 * par[3:4] + par[4:5]).astype(BF16)

    for copy in halo_copies + stat_copies + stat_copies2:
        copy.wait_send()
    for group in (weight_copies, moves, to_x, to_y, via_x, via_y):
        for copy in group.values():
            copy.wait_send()
    for group in (half_x, half_y, full_x, full_y, back):
        for copy in group.values():
            copy.wait_send()


def fused_shards(
    layer_input,
    doc_ids,
    routes,
    route_weight,
    pool_weight,
    pool_scale,
    norm1_gain,
    norm1_bias,
    expert_gate,
    expert_up,
    expert_down,
    shared_gate,
    shared_up,
    shared_down,
    norm2_gain,
    norm2_bias,
):
    rows, width = layer_input.shape
    experts = lax.axis_size("sp")
    tps = lax.axis_size("tp")
    top = routes.shape[1]
    cap = (rows * top * 11 + 8 * experts - 1) // (8 * experts)
    pad = -(-cap // 16) * 16
    hidden = expert_gate.shape[2]
    shared = shared_gate.shape[1]
    cols = jnp.concatenate(
        [doc_ids.astype(F32)[:, None], routes.astype(F32), route_weight.astype(F32)], axis=1
    )
    cols = jnp.pad(cols, ((0, 0), (0, LANES - cols.shape[1])))
    own = lax.dynamic_slice_in_dim(
        jnp.stack([pool_scale, norm1_gain, norm1_bias]), lax.axis_index("tp") * width, width, 1
    )
    par = jnp.concatenate([own, norm2_gain[None], norm2_bias[None]], axis=0)
    par = jnp.pad(par, ((0, 8 - par.shape[0]), (0, 0)))
    slots = (experts, pad, width)
    half = (experts, pad, width // 2)
    copies = 2 + 3 * (experts - 1) + 2 * (tps - 1) + 8 * (experts // 2)
    vmem = pl.BlockSpec(memory_space=pltpu.VMEM)
    hbm = pl.BlockSpec(memory_space=pl.ANY)
    return pl.pallas_call(
        functools.partial(fused_kernel, (experts, tps, cap, pad, WINDOWS)),
        out_shape=jax.ShapeDtypeStruct((rows, width), BF16),
        in_specs=[vmem] * 3 + [hbm] * 7,
        out_specs=vmem,
        scratch_shapes=[
            pltpu.VMEM((width, width), BF16),
            pltpu.VMEM((tps, width, hidden), BF16),
            pltpu.VMEM((tps, width, hidden), BF16),
            pltpu.VMEM((tps, hidden, width), BF16),
            pltpu.VMEM((tps, width, shared), BF16),
            pltpu.VMEM((tps, width, shared), BF16),
            pltpu.VMEM((tps, shared, width), BF16),
            pltpu.VMEM((HALO, width), BF16),
            pltpu.VMEM((HALO, LANES), F32),
            pltpu.VMEM((experts * pad, rows), BF16),
            pltpu.VMEM((experts, 8, LANES), F32),
            pltpu.VMEM((experts, 8, LANES), F32),
            pltpu.VMEM((2, 8, rows), F32),
            pltpu.VMEM((2, tps, 8, rows), F32),
            pltpu.VMEM((rows, width), BF16),
            pltpu.VMEM(slots, BF16),
            pltpu.VMEM((tps,) + slots, BF16),
            pltpu.VMEM((tps,) + slots, BF16),
            pltpu.VMEM(slots, F32),
            pltpu.VMEM(half, BF16),
            pltpu.VMEM(half, BF16),
            pltpu.VMEM(slots, BF16),
            pltpu.VMEM(slots, BF16),
            pltpu.VMEM(slots, BF16),
            pltpu.VMEM(slots, BF16),
            pltpu.SemaphoreType.DMA((copies,)),
            pltpu.SemaphoreType.DMA((copies,)),
            pltpu.SemaphoreType.DMA((1 + 6 * tps,)),
        ],
        compiler_params=pltpu.CompilerParams(
            collective_id=0, has_side_effects=True, vmem_limit_bytes=60 * 1024 * 1024
        ),
    )(
        layer_input,
        cols,
        par,
        pool_weight,
        expert_gate,
        expert_up,
        expert_down,
        shared_gate,
        shared_up,
        shared_down,
    )


def layer(*arrays):
    layer_input, pool_weight = arrays[0], arrays[4]
    one_group_each = layer_input.shape[1] == pool_weight.shape[1]
    if one_group_each and lax.axis_size("tp") == 4 and lax.axis_size("sp") % 2 == 0:
        return fused_shards(*arrays)
    return shards(*arrays)


def solution(mesh):
    in_specs = (
        P("sp", "tp"),
        P("sp"),
        P("sp", None),
        P("sp", None),
        P(),
        P(),
        P(),
        P(),
        P("sp", None, "tp"),
        P("sp", None, "tp"),
        P("sp", "tp", None),
        P(None, "tp"),
        P(None, "tp"),
        P("tp", None),
        P("tp"),
        P("tp"),
    )
    out_specs = P("sp", "tp")
    return jax.shard_map(layer, mesh=mesh, in_specs=in_specs, out_specs=out_specs, check_vma=False)
```

profile of v0, /device:TPU:0, one launch (start us, length us, event | category | flops | bytes accessed | tf_op | source)
XLA Modules:
  0.0 91.6 jit_solution(10746224243874342861)
XLA Ops:
  0.0 0.7 convert_element_type.10
  0.7 0.7 convert_element_type.11
  1.4 0.7 pad_maximum_fusion
  2.1 0.8 fusion.1
  2.8 1.3 %select_maximum_fusion.par_ref = f32[8,512]{1,0:T(8,128)} fusion(f32[1,512]{1,0:T(1,128)} %bitcast.10, f32[1,512]{1,0:T(1,128)} %bitcast.11, f32[3,512]{1,0:T(4,128)S(1)} %fusion.1), kind=kLoop, calls=%fused_computation.3 | loop fusion | flops 24576 | bytes 26624 | tf_op jit(solution)/shard_map/concatenate | solution.py:540
  4.2 0.1 copy.22
  4.3 0.7 pad.8.cols_ref
  5.0 85.0 %shard_map.154 = bf16[256,512]{1,0:T(8,128)(2,1)} custom-call(bf16[256,512]{1,0:T(8,128)(2,1)} %x_ref.1, f32[256,128]{1,0:T(8,128)} %pad.8.cols_ref, f32[8,512]{1,0:T(8,128)} %select_maximum_fusion.par_ref, bf16[4,512,512]{2,1,0:T(8,128)(2,1)} %pool_hbm.1, bf16[1,2048,512]{2,1,0:T(8,128)(2,1)} %gate_hbm.1, bf16[1,2048,512]{2,1,0:T(8,128)(2,1)} %up_hbm.1, ...), custom_call_target="tpu_custom_call" | custom-call | tf_op jit(solution)/shard_map/pallas_call | solution.py:547
  89.9 1.7 %copy.24 = bf16[256,512]{1,0:T(8,128)(2,1)} copy(bf16[256,512]{1,0:T(8,128)(2,1)} %shard_map.154) | data formatting | bytes 524288
where the time goes:
time: 91.9 us; the launch traced here: 91.6 us
  Pallas kernels  85 us (92%)
  other arithmetic  4.16 us (5%)
  local copies, waits for them, and re-layouts  2.47 us (3%)
    pallas_call x1, Pallas kernels, fused_shards(): pl.pallas_call(functools.partial(fused_kernel, (experts, tps, cap, pad, W...  85 us

commit v1 on v0

v1 whole, which is shorter than its diff:
```python
import functools

import jax
import jax.numpy as jnp
from jax import lax
from jax.experimental import pallas as pl
from jax.experimental.pallas import tpu as pltpu
from jax.sharding import PartitionSpec as P

WINDOWS = (2, 4, 8, 16)
HALO_ROWS = 15
RESIDUAL_SCALE = 2.0**0.5
NORM_EPS = 1e-05


def shifted(shard, axis, by):
    size = lax.axis_size(axis)
    pairs = [(i, i + by) for i in range(size) if 0 <= i + by < size]
    return lax.ppermute(shard, axis, pairs)


def pooled_groups(extended, marks, halo_rows):
    length = extended.shape[0] - halo_rows
    group_width = extended.shape[1] // len(WINDOWS)
    own_mark = marks[halo_rows:]
    values = extended.astype(jnp.float32)
    outputs = []
    for group_index, window in enumerate(WINDOWS):
        section = values[:, group_index * group_width : (group_index + 1) * group_width]
        running = jnp.zeros((length, group_width), jnp.float32)
        members = jnp.zeros((length, 1), jnp.float32)
        for offset in range(window):
            first_row = halo_rows - offset
            inside = (marks[first_row : first_row + length] == own_mark).astype(jnp.float32)[
                :, None
            ]
            running = running + inside * section[first_row : first_row + length]
            members = members + inside
        outputs.append(running / members - section[halo_rows:])
    return jnp.concatenate(outputs, axis=1).astype(jnp.bfloat16)


def layer_norm_rows(values, gain, bias):
    row_mean = jnp.mean(values, axis=1, keepdims=True)
    row_var = jnp.mean(values * values, axis=1, keepdims=True) - row_mean * row_mean
    return (values - row_mean) * lax.rsqrt(row_var + NORM_EPS) * gain + bias


def shards(
    layer_input,
    doc_ids,
    routes,
    route_weight,
    pool_weight,
    pool_scale,
    norm1_gain,
    norm1_bias,
    expert_gate,
    expert_up,
    expert_down,
    shared_gate,
    shared_up,
    shared_down,
    norm2_gain,
    norm2_bias,
):
    tokens_here = layer_input.shape[0]
    width_here = layer_input.shape[1]
    doc_marks = (doc_ids + 1).astype(jnp.bfloat16)
    tail_rows, tail_marks = shifted(
        (layer_input[tokens_here - HALO_ROWS :], doc_marks[tokens_here - HALO_ROWS :]), "sp", 1
    )
    extended = jnp.concatenate([tail_rows, layer_input], axis=0)
    marks = jnp.concatenate([tail_marks, doc_marks]).astype(jnp.float32)
    whole = lax.all_gather(extended, "tp", axis=1, tiled=True)
    model_width = whole.shape[1]
    mixed = pooled_groups(whole, marks, HALO_ROWS)
    groups = pool_weight.shape[0]
    group_width = pool_weight.shape[1]
    projected = jnp.einsum(
        "tgc,gcd->tgd",
        mixed.reshape(tokens_here, groups, group_width),
        pool_weight,
        preferred_element_type=jnp.float32,
    ).reshape(tokens_here, model_width)
    first = RESIDUAL_SCALE * whole[HALO_ROWS:].astype(jnp.float32) + projected * pool_scale
    normed = layer_norm_rows(first, norm1_gain, norm1_bias).astype(jnp.bfloat16)
    top = routes.shape[1]
    experts_all = lax.axis_size("sp")
    capacity = (tokens_here * top * 11 + 8 * experts_all - 1) // (8 * experts_all)
    flat_routes = routes.reshape(-1)
    one_hot = (flat_routes[:, None] == jnp.arange(experts_all, dtype=jnp.int32)[None, :]).astype(
        jnp.int32
    )
    ranks = jnp.sum((jnp.cumsum(one_hot, axis=0) - one_hot) * one_hot, axis=1)
    destination = flat_routes * capacity + ranks
    picked_rows = jnp.repeat(normed, top, axis=0)
    send_buffer = (
        jnp.zeros((experts_all * capacity, model_width), jnp.bfloat16)
        .at[destination]
        .set(picked_rows)
    )
    slot_grid = send_buffer.reshape(experts_all, capacity, model_width)
    own_columns = lax.dynamic_slice_in_dim(
        slot_grid, lax.axis_index("tp") * width_here, width_here, 2
    )
    moved = lax.all_to_all(own_columns, "sp", split_axis=0, concat_axis=0, tiled=True)
    arrived = lax.all_gather(moved, "tp", axis=2, tiled=True)
    arrived_rows = arrived.reshape(-1, model_width)
    gate_part = jnp.dot(arrived_rows, expert_gate[0], preferred_element_type=jnp.float32)
    up_part = jnp.dot(arrived_rows, expert_up[0], preferred_element_type=jnp.float32)
    expert_hidden = (jax.nn.silu(gate_part) * up_part).astype(jnp.bfloat16)
    routed_partial = jnp.dot(expert_hidden, expert_down[0], preferred_element_type=jnp.float32)
    shared_gate_part = jnp.dot(normed, shared_gate, preferred_element_type=jnp.float32)
    shared_up_part = jnp.dot(normed, shared_up, preferred_element_type=jnp.float32)
    shared_hidden = (jax.nn.silu(shared_gate_part) * shared_up_part).astype(jnp.bfloat16)
    shared_partial = jnp.dot(shared_hidden, shared_down, preferred_element_type=jnp.float32)
    routed_sum, shared_sum = (
        lax.psum_scatter(
            routed_partial.astype(jnp.bfloat16), "tp", scatter_dimension=1, tiled=True
        ).astype(jnp.float32),
        lax.psum_scatter(
            shared_partial.astype(jnp.bfloat16), "tp", scatter_dimension=1, tiled=True
        ).astype(jnp.float32),
    )
    routed_here = routed_sum.astype(jnp.bfloat16).reshape(experts_all, capacity, width_here)
    returned = lax.all_to_all(routed_here, "sp", split_axis=0, concat_axis=0, tiled=True)
    returned_rows = returned.reshape(experts_all * capacity, width_here)
    picked_out = (
        returned_rows[destination].astype(jnp.float32).reshape(tokens_here, top, width_here)
    )
    routed_mix = jnp.sum(picked_out * route_weight[:, :, None], axis=1)
    own_normed = lax.dynamic_slice_in_dim(
        normed, lax.axis_index("tp") * width_here, width_here, 1
    ).astype(jnp.float32)
    second = RESIDUAL_SCALE * own_normed + routed_mix + shared_sum
    row_total, row_squares = lax.psum(
        (jnp.sum(second, axis=1), jnp.sum(second * second, axis=1)), "tp"
    )
    row_mean = row_total / model_width
    row_var = row_squares / model_width - row_mean * row_mean
    scaled = (second - row_mean[:, None]) * lax.rsqrt(row_var + NORM_EPS)[:, None]
    return (scaled * norm2_gain + norm2_bias).astype(jnp.bfloat16)


MESH_ID = pl.DeviceIdType.MESH
HALO = 16
LANES = 128
F32 = jnp.float32
BF16 = jnp.bfloat16
ORDER = (
    "G0", "G1", "R0", "G2", "R1", "G3", "R2", "R3", "G4", "G5", "D3", "E0", "S0", "S1",
    "H0", "E1", "H1", "R4", "R5", "G6", "G7", "E2", "S4", "S5", "R6", "H2", "R7", "F4",
    "F5", "E3", "S6", "S7", "S2", "S3", "T4", "T5", "H3", "F6", "F7", "F2", "F3", "F1",
    "F0", "T6", "T7", "T2", "T3", "T1", "M2", "T0", "M1", "M3", "M0",
)


def fused_kernel(
    dims,
    x_hbm,
    doc_hbm,
    route_hbm,
    weight_hbm,
    scale_hbm,
    gain1_hbm,
    bias1_hbm,
    gain2_hbm,
    bias2_hbm,
    pool_hbm,
    gate_hbm,
    up_hbm,
    down_hbm,
    sgate_hbm,
    sup_hbm,
    sdown_hbm,
    out_ref,
    x_ref,
    doc_ref,
    route_ref,
    weight_ref,
    scale_ref,
    gain1_ref,
    bias1_ref,
    gain2_ref,
    bias2_ref,
    pool_w,
    gate_w,
    up_w,
    down_w,
    sgate_w,
    sup_w,
    sdown_w,
    halo_x,
    halo_s,
    halo_c,
    disp,
    disp_t,
    picks,
    wsend,
    wrecv,
    stat_send,
    stat_recv,
    acc,
    sbuf,
    xs,
    pbuf,
    pown,
    rdx,
    rdy,
    fx,
    fy,
    rsend,
    rback,
    send_sems,
    recv_sems,
    load_sems,
):
    experts, tps, cap, pad, windows = dims
    rows, width = x_ref.shape
    half = width // 2
    chips = experts // 2
    model_width = width * tps
    sp = lax.axis_index("sp")
    tp = lax.axis_index("tp")
    chip = sp // 2
    core = sp % 2
    xn = tp + 1 - 2 * (tp % 2)
    yn = lax.rem(tp + 2, tps)
    diag = xn + 2 - 4 * (xn // 2)
    at_q = (tp, xn, yn, diag)
    bits = [1 << i for i in range(chips.bit_length() - 1)]

    def peer(j):
        across = 0
        for bit in bits:
            own = (chip // bit) % 2
            across = across + bit * (1 - own if (j // 2) & bit else own)
        return across * 2 + (1 - core if j % 2 else core)

    counter = [0]

    def remote(src, dst, device):
        k = counter[0]
        counter[0] += 1
        return pltpu.make_async_remote_copy(
            src_ref=src,
            dst_ref=dst,
            send_sem=send_sems.at[k],
            recv_sem=recv_sems.at[k],
            device_id=device,
            device_id_type=MESH_ID,
        )

    barrier = pltpu.get_barrier_semaphore()
    for q in range(1, tps):
        pl.semaphore_signal(barrier, inc=1, device_id=(sp, at_q[q]), device_id_type=MESH_ID)
    for j in range(1, experts):
        pl.semaphore_signal(barrier, inc=1, device_id=(peer(j), tp), device_id_type=MESH_ID)

    loads = {}
    load_count = [0]

    def load(name, src, dst):
        k = load_count[0]
        load_count[0] += 1
        copy = pltpu.make_async_copy(src, dst, load_sems.at[k])
        copy.start()
        loads.setdefault(name, []).append(copy)

    def loaded(name):
        for copy in loads[name]:
            copy.wait()

    def of_q(ref, q):
        return ref[:, pl.ds(pl.multiple_of(at_q[q] * width, width), width)]

    own_block = pl.ds(pl.multiple_of(tp * width, width), width)
    load("x", x_hbm, x_ref)
    load("doc", doc_hbm, doc_ref)
    load("route", route_hbm, route_ref)
    load("route", weight_hbm, weight_ref)
    load("pool", pool_hbm.at[tp], pool_w)
    load("pool", scale_hbm.at[:, own_block], scale_ref)
    load("norm", gain1_hbm, gain1_ref)
    load("norm", bias1_hbm, bias1_ref)
    load("norm", gain2_hbm, gain2_ref)
    load("norm", bias2_hbm, bias2_ref)
    for q in range(tps):
        block = pl.ds(pl.multiple_of(at_q[q] * width, width), width)
        load("in", gate_hbm.at[0, block, :], gate_w.at[q])
        load("in", up_hbm.at[0, block, :], up_w.at[q])
        load("in", sgate_hbm.at[block, :], sgate_w.at[q])
        load("in", sup_hbm.at[block, :], sup_w.at[q])
        load("down", down_hbm.at[0, :, block], down_w.at[q])
        load("down", sdown_hbm.at[:, block], sdown_w.at[q])

    loaded("doc")
    sub8 = lax.broadcasted_iota(jnp.int32, (8, rows), 0)
    doc_row = jnp.where(sub8 == 0, doc_ref[...].astype(F32), 0.0)
    docs = jnp.broadcast_to(doc_row.T[:, 0:1], (rows, LANES))
    halo_s[...] = docs[rows - HALO :]
    loaded("x")

    following = lax.rem(sp + 1, experts)
    halo_copies = [
        remote(x_ref.at[pl.ds(rows - HALO, HALO)], halo_x, (following, tp)),
        remote(halo_s, halo_c, (following, tp)),
    ]
    with jax.named_scope("barrier"):
        pl.semaphore_wait(barrier, tps - 1 + experts - 1)

    @pl.when(sp < experts - 1)
    def _():
        for copy in halo_copies:
            copy.start()

    window = jnp.int32(windows[0])
    for index in range(1, len(windows)):
        window = jnp.where(tp == index, windows[index], window)

    def pooled(values, marks):
        running = values
        members = jnp.ones(marks.shape, F32)
        step = 1
        while step < max(windows):
            same = (marks == pltpu.roll(marks, step, 0)) & (step < window)
            running = running + jnp.where(same[:, 0:1], pltpu.roll(running, step, 0), 0.0)
            members = members + jnp.where(same, pltpu.roll(members, step, 0), 0.0)
            step *= 2
        return (running / members[:, 0:1] - values).astype(BF16)

    def projected(values, mixed):
        product = jnp.dot(mixed, pool_w[...], preferred_element_type=F32)
        return (2.0**0.5) * values + product * scale_ref[...]

    value = x_ref[...].astype(F32)
    mixed = pooled(value, docs)
    loaded("pool")
    first = projected(value, mixed)
    sums = [
        jnp.sum(first, axis=1, keepdims=True),
        jnp.sum(first * first, axis=1, keepdims=True),
    ]

    lane = lax.broadcasted_iota(jnp.int32, (rows, LANES), 1)
    loaded("route")
    routes = route_ref[...].astype(F32)
    weights = weight_ref[...]
    table = jnp.where(
        sub8 == 0,
        routes[0:1],
        jnp.where(
            sub8 == 1,
            routes[1:2],
            jnp.where(sub8 == 2, weights[0:1], jnp.where(sub8 == 3, weights[1:2], 0.0)),
        ),
    )
    cols = table.T
    route = [(cols[:, k : 1 + k] + 0.5).astype(jnp.int32) for k in range(2)]
    named = [lane == route[k] for k in range(2)]
    count = named[0].astype(F32) + named[1].astype(F32)
    earlier = (
        lax.broadcasted_iota(jnp.int32, (rows, rows), 0)
        > lax.broadcasted_iota(jnp.int32, (rows, rows), 1)
    ).astype(F32)
    rank = jnp.dot(earlier.astype(BF16), count.astype(BF16), preferred_element_type=F32)
    differs = jnp.where(lane % 2 == core, 0, 1)
    for bit in bits:
        differs = differs + jnp.where((lane // (2 * bit)) % 2 == (chip // bit) % 2, 0, 2 * bit)
    place = (rank + 0.5).astype(jnp.int32) + differs * pad
    dest = [
        jnp.sum(jnp.where(named[k], place, 0).astype(F32), axis=1, keepdims=True) for k in range(2)
    ]
    wide = (place + differs * (LANES - pad)).astype(F32)
    dest_wide = [
        jnp.sum(jnp.where(named[k], wide, 0.0), axis=1, keepdims=True) for k in range(2)
    ]
    both = jnp.where(lane == 0, dest[0], jnp.where(lane == 1, dest[1], 0.0))
    both_rows = both.T
    slot_row = lax.broadcasted_iota(jnp.int32, (experts * pad, rows), 0)
    dest_row = [(both_rows[k : k + 1, :] + 0.5).astype(jnp.int32) for k in range(2)]
    disp[...] = jnp.where(
        (slot_row == dest_row[0]) | (slot_row == dest_row[1]), 1.0, 0.0
    ).astype(BF16)
    dest_col = [(dest[k] + 0.5).astype(jnp.int32) for k in range(2)]

    @pl.when(sp > 0)
    def _():
        with jax.named_scope("halo_wait"):
            for copy in halo_copies:
                copy.wait_recv()

    halo_docs = jnp.where(sp == 0, -1.0, halo_c[...])
    early = jnp.concatenate([halo_x[...].astype(F32), value[:HALO]], axis=0)
    early_docs = jnp.concatenate([halo_docs, docs[:HALO]], axis=0)
    early_mixed = pooled(early, early_docs)[HALO:]
    early_first = projected(value[:HALO], early_mixed)
    first = jnp.concatenate([early_first, first[HALO:]], axis=0)
    sums = [
        jnp.concatenate([jnp.sum(early_first, axis=1, keepdims=True), sums[0][HALO:]], axis=0),
        jnp.concatenate(
            [jnp.sum(early_first * early_first, axis=1, keepdims=True), sums[1][HALO:]], axis=0
        ),
    ]
    centred = (first - sums[0] / width).astype(BF16)
    acc[...] = first

    def exchange_start(total, squares, slot):
        tile = jnp.where(lane == 0, total, jnp.where(lane == 1, squares, 0.0))
        own = tile.T[0:8]
        stat_send[slot] = own
        copies = []
        for q in range(1, tps):
            copies.append(remote(stat_send.at[slot], stat_recv.at[slot, q], (sp, at_q[q])))
            copies[-1].start()
        return own, copies

    def exchange_end(own, copies, slot):
        with jax.named_scope("stat_wait%d" % slot):
            for copy in copies:
                copy.wait_recv()
        shares = [own] + [stat_recv[slot, q] for q in range(1, tps)]
        whole = shares[0]
        for q in range(1, tps):
            whole = whole + shares[q]
        mean = whole[0:1] / model_width
        var = whole[1:2] / model_width - mean * mean
        inverse = lax.rsqrt(var + 1e-5)
        back = jnp.where(sub8 == 0, mean, jnp.where(sub8 == 1, inverse, 0.0)).T
        shifts = [share[0:1] / width - mean for share in shares]
        return back[:, 0:1], back[:, 1:2], inverse, shifts

    moves, to_x, to_y, via_x, via_y = {}, {}, {}, {}, {}
    half_x, half_y, full_x, full_y, back = {}, {}, {}, {}, {}
    weight_copies = {}
    low, high = pl.ds(0, half), pl.ds(half, half)

    def unit(ref, q, j, columns=None):
        if columns is None:
            return ref.at[q, j, pl.ds(0, cap)]
        return ref.at[q, j, pl.ds(0, cap), columns]

    def plain(ref, j):
        return ref.at[j, pl.ds(0, cap)]

    def gather(j):
        if j:
            with jax.named_scope("w_moves#%d" % j):
                moves[j].wait_recv()
        to_x[j] = remote(unit(xs, 0, j), unit(xs, 1, j), (sp, xn))
        to_x[j].start()
        to_y[j] = remote(unit(xs, 0, j), unit(xs, 2, j), (sp, yn))
        to_y[j].start()

    def relay(j):
        with jax.named_scope("w_to#%d" % j):
            to_x[j].wait_recv()
        via_y[j] = remote(unit(xs, 1, j, low), unit(xs, 3, j, low), (sp, yn))
        via_y[j].start()
        with jax.named_scope("w_to#%d" % j):
            to_y[j].wait_recv()
        via_x[j] = remote(unit(xs, 2, j, high), unit(xs, 3, j, high), (sp, xn))
        via_x[j].start()

    expert_started = []
    partials = {}

    def expert(c):
        for j in (2 * c, 2 * c + 1):
            with jax.named_scope("w_via#%d" % j):
                via_x[j].wait_recv()
                via_y[j].wait_recv()
                if j:
                    weight_copies[j].wait_recv()
        if not expert_started:
            loaded("in")
        size = 2 * pad
        tiles = [wrecv[2 * c + b].T[0:pad] for b in range(2)]
        slot = jnp.concatenate(tiles, axis=0)
        acts = []
        for q in range(tps):
            raw = xs[q, 2 * c : 2 * c + 2].reshape(size, width).astype(F32)
            raw = (raw + slot[:, 3 + q : 4 + q]) * slot[:, 2:3]
            acts.append((raw * of_q(gain1_ref, q) + of_q(bias1_ref, q)).astype(BF16))

        def project(w):
            total = jnp.dot(acts[0], w[0], preferred_element_type=F32)
            for q in range(1, tps):
                total = total + jnp.dot(acts[q], w[q], preferred_element_type=F32)
            return total

        hidden = (jax.nn.silu(project(gate_w)) * project(up_w) * slot[:, 0:1]).astype(BF16)
        shared = (jax.nn.silu(project(sgate_w)) * project(sup_w) * slot[:, 1:2]).astype(BF16)
        if not expert_started:
            loaded("down")
            expert_started.append(True)

        def partial(q):
            return jnp.dot(hidden, down_w[q], preferred_element_type=F32) + jnp.dot(
                shared, sdown_w[q], preferred_element_type=F32
            )

        two = slice(2 * c, 2 * c + 2)
        pbuf[3, two] = partial(3).astype(BF16).reshape(2, pad, width)
        partials[c] = partial

    def hand_over(c):
        two = slice(2 * c, 2 * c + 2)
        pbuf[1, two] = partials[c](1).astype(BF16).reshape(2, pad, width)
        pbuf[2, two] = partials[c](2).astype(BF16).reshape(2, pad, width)
        pown[two] = partials[c](0).reshape(2, pad, width)

    def spread(j):
        half_x[j] = remote(unit(pbuf, 3, j, low), plain(rdx, j), (sp, xn))
        half_x[j].start()
        half_y[j] = remote(unit(pbuf, 3, j, high), plain(rdy, j), (sp, yn))
        half_y[j].start()

    def fold(j):
        with jax.named_scope("w_half#%d" % j):
            half_x[j].wait_recv()
        pbuf[2, j, :, :half] = (pbuf[2, j, :, :half].astype(F32) + rdx[j].astype(F32)).astype(BF16)
        full_y[j] = remote(unit(pbuf, 2, j), plain(fy, j), (sp, yn))
        full_y[j].start()
        with jax.named_scope("w_half#%d" % j):
            half_y[j].wait_recv()
        pbuf[1, j, :, half:] = (pbuf[1, j, :, half:].astype(F32) + rdy[j].astype(F32)).astype(BF16)
        full_x[j] = remote(unit(pbuf, 1, j), plain(fx, j), (sp, xn))
        full_x[j].start()

    def turn(j):
        with jax.named_scope("w_full#%d" % j):
            full_x[j].wait_recv()
            full_y[j].wait_recv()
        total = (pown[j] + fx[j].astype(F32) + fy[j].astype(F32)).astype(BF16)
        if j == 0:
            rback[0] = total
        else:
            rsend[j] = total
            back[j] = remote(plain(rsend, j), plain(rback, j), (peer(j), tp))
            back[j].start()

    def merge(c):
        for j in (2 * c, 2 * c + 1):
            if j:
                with jax.named_scope("w_back#%d" % j):
                    back[j].wait_recv()
        slots = rback[2 * c : 2 * c + 2].reshape(2 * pad, width)
        inner = lax.broadcasted_iota(jnp.int32, (2, pad, width), 1).reshape(2 * pad, width)
        slots = jnp.where(inner < cap, slots.astype(F32), 0.0).astype(BF16)
        acc[...] += jnp.dot(disp_t[c], slots, preferred_element_type=F32)

    own1, stat_copies = exchange_start(sums[0], sums[1], 0)
    inner_chip = ((chip + 1) // 2) % 2 == 1
    for c in range(chips):
        part = jnp.dot(
            disp[c * 2 * pad : (c + 1) * 2 * pad, :], centred, preferred_element_type=F32
        ).astype(BF16)
        for b in range(2):
            j = 2 * c + b
            piece = part[b * pad : (b + 1) * pad]
            if j == 0:
                xs[0, 0] = piece
                gather(0)
            else:
                sbuf[j] = piece
                moves[j] = remote(plain(sbuf, j), xs.at[0, j, pl.ds(0, cap)], (peer(j), tp))
                if c < 2:
                    moves[j].start()

    @pl.when(inner_chip)
    def _():
        for j in (6, 7):
            moves[j].start()

    pick_lane = lax.broadcasted_iota(jnp.int32, (rows, experts * LANES), 1)
    for k in range(2):
        spot = (dest_wide[k] + 0.5).astype(jnp.int32)
        picks[k * rows : (k + 1) * rows] = jnp.where(pick_lane == spot, 1.0, 0.0).astype(BF16)
    with jax.named_scope("G1"):
        gather(1)
    mean, inverse, inverse_row, shifts = exchange_end(own1, stat_copies, 0)

    def slot_rows(weight_row, flag):
        out = jnp.where(sub8 == 0, weight_row, jnp.where(sub8 == 1, flag, 0.0))
        out = jnp.where(sub8 == 2, inverse_row, out)
        for q in range(tps):
            out = jnp.where(sub8 == 3 + q, shifts[q], out)
        return out

    left = jnp.concatenate([slot_rows(weights[0:1], 1.0), slot_rows(weights[1:2], 0.0)], axis=1)
    slot_values = jnp.zeros((8, experts * LANES), F32)
    for _ in range(3):
        piece = left.astype(BF16)
        slot_values = slot_values + jnp.dot(piece, picks[...], preferred_element_type=F32)
        left = left - piece.astype(F32)
    for j in range(experts):
        tile = slot_values[:, j * LANES : (j + 1) * LANES]
        if j == 0:
            wrecv[0] = tile
        else:
            wsend[j] = tile
            weight_copies[j] = remote(wsend.at[j], wrecv.at[j], (peer(j), tp))
            weight_copies[j].start()

    @pl.when(inner_chip)
    def _():
        for j in (4, 5):
            moves[j].start()

    @pl.when(jnp.logical_not(inner_chip))
    def _():
        for j in (4, 5):
            moves[j].start()

    loaded("norm")
    normed = ((acc[...] - mean) * inverse * of_q(gain1_ref, 0) + of_q(bias1_ref, 0)).astype(BF16)
    acc[...] = (2.0**0.5) * normed.astype(F32)
    slot_lane = lax.broadcasted_iota(jnp.int32, (rows, 2 * pad), 1)
    for c in range(chips):
        here = slot_lane + c * 2 * pad
        disp_t[c] = jnp.where((here == dest_col[0]) | (here == dest_col[1]), 1.0, 0.0).astype(BF16)

    def depart(pair):
        @pl.when(jnp.logical_not(inner_chip))
        def _():
            for j in (2 * pair, 2 * pair + 1):
                moves[j].start()

    stages = {
        "D": depart, "G": gather, "R": relay, "E": expert, "H": hand_over, "S": spread, "F": fold, "T": turn, "M": merge
    }
    for step in ORDER:
        if step in ("G0", "G1"):
            continue
        with jax.named_scope(step):
            stages[step[0]](int(step[1:]))

    second = acc[...]
    own2, stat_copies2 = exchange_start(
        jnp.sum(second, axis=1, keepdims=True), jnp.sum(second * second, axis=1, keepdims=True), 1
    )
    mean2, inverse2, _, _ = exchange_end(own2, stat_copies2, 1)
    with jax.named_scope("final"):
        out_ref[...] = ((second - mean2) * inverse2 * gain2_ref[...] + bias2_ref[...]).astype(BF16)

    @pl.when(sp < experts - 1)
    def _():
        for copy in halo_copies:
            copy.wait_send()

    for copy in stat_copies + stat_copies2:
        copy.wait_send()
    for group in (weight_copies, moves, to_x, to_y, via_x, via_y):
        for copy in group.values():
            copy.wait_send()
    for group in (half_x, half_y, full_x, full_y, back):
        for copy in group.values():
            copy.wait_send()


def fused_shards(
    layer_input,
    doc_ids,
    routes,
    route_weight,
    pool_weight,
    pool_scale,
    norm1_gain,
    norm1_bias,
    expert_gate,
    expert_up,
    expert_down,
    shared_gate,
    shared_up,
    shared_down,
    norm2_gain,
    norm2_bias,
):
    rows, width = layer_input.shape
    experts = lax.axis_size("sp")
    tps = lax.axis_size("tp")
    top = routes.shape[1]
    cap = (rows * top * 11 + 8 * experts - 1) // (8 * experts)
    pad = -(-cap // 16) * 16
    hidden = expert_gate.shape[2]
    shared = shared_gate.shape[1]
    slots = (experts, pad, width)
    half = (experts, pad, width // 2)
    copies = 2 + 3 * (experts - 1) + 2 * (tps - 1) + 8 * experts
    vmem = pl.BlockSpec(memory_space=pltpu.VMEM)
    hbm = pl.BlockSpec(memory_space=pl.ANY)
    return pl.pallas_call(
        functools.partial(fused_kernel, (experts, tps, cap, pad, WINDOWS)),
        out_shape=jax.ShapeDtypeStruct((rows, width), BF16),
        in_specs=[hbm] * 16,
        out_specs=vmem,
        scratch_shapes=[
            pltpu.VMEM((rows, width), BF16),
            pltpu.VMEM((1, rows), jnp.int32),
            pltpu.VMEM((top, rows), jnp.int32),
            pltpu.VMEM((top, rows), F32),
            pltpu.VMEM((1, width), F32),
            pltpu.VMEM((1, tps * width), F32),
            pltpu.VMEM((1, tps * width), F32),
            pltpu.VMEM((1, width), F32),
            pltpu.VMEM((1, width), F32),
            pltpu.VMEM((width, width), BF16),
            pltpu.VMEM((tps, width, hidden), BF16),
            pltpu.VMEM((tps, width, hidden), BF16),
            pltpu.VMEM((tps, hidden, width), BF16),
            pltpu.VMEM((tps, width, shared), BF16),
            pltpu.VMEM((tps, width, shared), BF16),
            pltpu.VMEM((tps, shared, width), BF16),
            pltpu.VMEM((HALO, width), BF16),
            pltpu.VMEM((HALO, LANES), F32),
            pltpu.VMEM((HALO, LANES), F32),
            pltpu.VMEM((experts * pad, rows), BF16),
            pltpu.VMEM((experts // 2, rows, 2 * pad), BF16),
            pltpu.VMEM((top * rows, experts * LANES), BF16),
            pltpu.VMEM((experts, 8, LANES), F32),
            pltpu.VMEM((experts, 8, LANES), F32),
            pltpu.VMEM((2, 8, rows), F32),
            pltpu.VMEM((2, tps, 8, rows), F32),
            pltpu.VMEM((rows, width), F32),
            pltpu.VMEM(slots, BF16),
            pltpu.VMEM((tps,) + slots, BF16),
            pltpu.VMEM((tps,) + slots, BF16),
            pltpu.VMEM(slots, F32),
            pltpu.VMEM(half, BF16),
            pltpu.VMEM(half, BF16),
            pltpu.VMEM(slots, BF16),
            pltpu.VMEM(slots, BF16),
            pltpu.VMEM(slots, BF16),
            pltpu.VMEM(slots, BF16),
            pltpu.SemaphoreType.DMA((copies,)),
            pltpu.SemaphoreType.DMA((copies,)),
            pltpu.SemaphoreType.DMA((10 + 6 * tps,)),
        ],
        compiler_params=pltpu.CompilerParams(
            collective_id=0, has_side_effects=True, vmem_limit_bytes=60 * 1024 * 1024
        ),
    )(
        layer_input,
        doc_ids.reshape(1, rows),
        routes.T,
        route_weight.T,
        pool_scale.reshape(1, -1),
        norm1_gain.reshape(1, -1),
        norm1_bias.reshape(1, -1),
        norm2_gain.reshape(1, -1),
        norm2_bias.reshape(1, -1),
        pool_weight,
        expert_gate,
        expert_up,
        expert_down,
        shared_gate,
        shared_up,
        shared_down,
    )


def layer(*arrays):
    layer_input, pool_weight = arrays[0], arrays[4]
    one_group_each = layer_input.shape[1] == pool_weight.shape[1]
    if one_group_each and lax.axis_size("tp") == 4 and lax.axis_size("sp") == 8:
        return fused_shards(*arrays)
    return shards(*arrays)


def solution(mesh):
    in_specs = (
        P("sp", "tp"),
        P("sp"),
        P("sp", None),
        P("sp", None),
        P(),
        P(),
        P(),
        P(),
        P("sp", None, "tp"),
        P("sp", None, "tp"),
        P("sp", "tp", None),
        P(None, "tp"),
        P(None, "tp"),
        P("tp", None),
        P("tp"),
        P("tp"),
    )
    out_specs = P("sp", "tp")
    return jax.shard_map(layer, mesh=mesh, in_specs=in_specs, out_specs=out_specs, check_vma=False)
```

time: 91.9 us -> 67.2 us (0.73)
  Pallas kernels: 85 us -> 65.4 us
  other arithmetic: 4.16 us -> 0 us
    pallas_call x1, Pallas kernels: 85 us -> 65.4 us  [fused_shards(): pl.pallas_call(functools.partial(fused_kernel, (experts, tps, cap, pad, W...]
    concatenate x2 -> x0, other arithmetic: 2 us -> none  [the longest x1 1.31 us: fused_shards(): par = jnp.concatenate([own, norm2_gain[None], norm2_bias[None]], axis=0)]
    convert_element_type x2 -> x0, other arithmetic: 1.36 us -> none  [the longest x1 0.68 us: fused_shards(): routes.astype(F32)]
where the time goes in v1:
time: 67.2 us; the launch traced here: 67.1 us
  Pallas kernels  65.4 us (97%)
  local copies, waits for them, and re-layouts  1.67 us (2%)
    pallas_call x1, Pallas kernels, fused_shards(): pl.pallas_call(functools.partial(fused_kernel, (experts, tps, cap, pad, W...  65.4 us
    unnamed x1, local copies, waits for them, and re-layouts  1.67 us

profile of v1, /device:TPU:0, one launch (start us, length us, event | category | flops | bytes accessed | tf_op | source)
XLA Modules:
  0.0 67.1 jit_solution(3249238932405445085)
XLA Ops:
  0.0 65.4 %shard_map.154 = bf16[256,512]{1,0:T(8,128)(2,1)} custom-call(bf16[256,512]{1,0:T(8,128)(2,1)} %x_hbm.1, s32[1,256]{1,0:T(1,128)} %bitcast.15, s32[2,256]{1,0:T(2,128)} %bitcast.11, f32[2,256]{1,0:T(2,128)} %bitcast.12, f32[1,2048]{1,0:T(1,128)} %bitcast.8, f32[1,2048]{1,0:T(1,128)} %bitcast.9, f32[1,2048]{1,0:T(1,128)} %bitcast.10, f32[1,512]{1,0:T(1,128)} %bitcast.13, ...), custom_call_target="tpu_custom_call" | custom-call | tf_op jit(solution)/shard_map/pallas_call | solution.py:694
  65.4 1.7 %copy.18 = bf16[256,512]{1,0:T(8,128)(2,1)} copy(bf16[256,512]{1,0:T(8,128)(2,1)} %shard_map.154) | data formatting | bytes 524288
